TPU v7x, 32 devices: a whole 2x2x4 slice. The times are simulated.
32 devices in a mesh: fs: 8 (over z, y), tp: 4 (over x, core).
Axes of the slice: x: 2, y: 2, z: 4, core: 2. Of those that a mesh axis runs over, the one named last changes fastest.
Arguments:
- inputs: bfloat16 [8192, 2304], P('fs'), may hold values from -6 to 6
- query_cot: bfloat16 [8192, 1024], P('fs', 'tp'), may hold values from -6 to 6
- head_out: bfloat16 [8192, 1024], P('fs', 'tp'), may hold values from -6 to 6
- out_cot: bfloat16 [8192, 2304], P('fs'), may hold values from -6 to 6
- query_factor: bfloat16 [2304, 192], P('fs'), may hold values from -2.5 to 2.5
- out_factor: bfloat16 [2304, 192], P('fs'), may hold values from -2.5 to 2.5
- query_master: float32 [2304, 1024], P('fs', 'tp'), may hold values from -0.125 to 0.125
- out_master: float32 [2304, 1024], P('fs', 'tp'), may hold values from -0.1875 to 0.1875
- query_first: float32 [192, 1024], P('fs', 'tp'), may hold values from -6 to 6
- query_second: float32 [192, 1024], P('fs', 'tp'), may hold values from 0.3 to 3
- out_first: float32 [192, 1024], P('fs', 'tp'), may hold values from -6 to 6
- out_second: float32 [192, 1024], P('fs', 'tp'), may hold values from 0.3 to 3
Outputs:
- query_step: float32 [2304, 1024], P('fs', 'tp')
- out_step: float32 [2304, 1024], P('fs', 'tp')
- query_copy: bfloat16 [2304, 1024], P(None, 'tp')
- out_copy: bfloat16 [2304, 1024], P(None, 'tp')
- query_first_new: float32 [192, 1024], P('fs', 'tp')
- query_second_new: float32 [192, 1024], P('fs', 'tp')
- out_first_new: float32 [192, 1024], P('fs', 'tp')
- out_second_new: float32 [192, 1024], P('fs', 'tp')
All inputs are finite; a program needn't handle non-finite values.
Results may differ from a plain program's by a relative error of at most 0.0065.
Values may be sent and summed in bfloat16 or wider, within the bound.
A program may use at most 64 MiB of HBM per device.

v0:
```python
import jax
import jax.numpy as jnp
from jax import lax
from jax.sharding import PartitionSpec as P

HEADS = 8
HEAD = 128
RANK = 192


beta_first = 0.8
beta_second = 0.95
adam_eps = 1e-08
learn_rate = 0.05
norm_eps = 1e-06
contract_rows = (((0,), (0,)), ((), ()))


def moment_update(normed, first_old, second_old):
    first_new = beta_first * first_old + (1.0 - beta_first) * normed
    second_new = beta_second * second_old + (1.0 - beta_second) * normed * normed
    direction = (first_new / (jnp.sqrt(second_new) + adam_eps)).astype(jnp.bfloat16)
    return (first_new, second_new, direction)


def slice_fold(source, factor_piece):
    return jnp.dot(source, factor_piece, preferred_element_type=jnp.float32)


def body(
    inputs,
    query_cot,
    head_out,
    out_cot,
    query_factor,
    out_factor,
    query_master,
    out_master,
    query_first,
    query_second,
    out_first,
    out_second,
):
    cot_proj = slice_fold(out_cot, lax.all_gather(out_factor, "fs", axis=0, tiled=True))
    grad_q = lax.psum_scatter(
        lax.dot_general(inputs, query_cot, contract_rows, preferred_element_type=jnp.float32),
        "fs",
        scatter_dimension=0,
        tiled=True,
    )
    term_q = lax.dot_general(
        query_factor.astype(jnp.float32), grad_q, contract_rows, precision=lax.Precision.HIGHEST
    )
    cot_low = cot_proj.astype(jnp.bfloat16)
    term_o = lax.dot_general(cot_low, head_out, contract_rows, preferred_element_type=jnp.float32)
    count_all = 2.0 * RANK * HEADS * HEAD
    whole_q, whole_o = lax.psum((term_q, term_o), "fs")
    sq_total = lax.psum(jnp.sum(whole_q * whole_q) + jnp.sum(whole_o * whole_o), "tp")
    rms_value = jnp.sqrt(sq_total / count_all + norm_eps)
    previous = (
        lax.all_gather(query_first, "fs", axis=0, tiled=True),
        lax.all_gather(query_second, "fs", axis=0, tiled=True),
        lax.all_gather(out_first, "fs", axis=0, tiled=True),
        lax.all_gather(out_second, "fs", axis=0, tiled=True),
    )
    moment_q, second_wq, full_q = moment_update(whole_q / rms_value, previous[0], previous[1])
    moment_o, second_wo, full_o = moment_update(whole_o / rms_value, previous[2], previous[3])
    own_rows = query_first.shape[0]
    row_start = lax.axis_index("fs") * own_rows
    first_q = lax.dynamic_slice_in_dim(moment_q, row_start, own_rows, 0)
    second_q = lax.dynamic_slice_in_dim(second_wq, row_start, own_rows, 0)
    first_o = lax.dynamic_slice_in_dim(moment_o, row_start, own_rows, 0)
    second_o = lax.dynamic_slice_in_dim(second_wo, row_start, own_rows, 0)
    query_step = jnp.dot(query_factor, full_q, preferred_element_type=jnp.float32)
    out_step = jnp.dot(out_factor, full_o, preferred_element_type=jnp.float32)
    copy_q = (query_master - learn_rate * query_step).astype(jnp.bfloat16)
    copy_o = (out_master - learn_rate * out_step).astype(jnp.bfloat16)
    query_copy, out_copy = (
        lax.all_gather(copy_q, "fs", axis=0, tiled=True),
        lax.all_gather(copy_o, "fs", axis=0, tiled=True),
    )
    return (query_step, out_step, query_copy, out_copy, first_q, second_q, first_o, second_o)


def solution(mesh):
    placed = (
        P("fs", None),
        P("fs", "tp"),
        P("fs", "tp"),
        P("fs", None),
        P("fs", None),
        P("fs", None),
        P("fs", "tp"),
        P("fs", "tp"),
        P("fs", "tp"),
        P("fs", "tp"),
        P("fs", "tp"),
        P("fs", "tp"),
    )
    return jax.shard_map(
        body,
        mesh=mesh,
        in_specs=placed,
        out_specs=(
            P("fs", "tp"),
            P("fs", "tp"),
            P(None, "tp"),
            P(None, "tp"),
            P("fs", "tp"),
            P("fs", "tp"),
            P("fs", "tp"),
            P("fs", "tp"),
        ),
        check_vma=False,
    )
```

profile of v0, /device:TPU:0, one launch (start us, length us, event | category | flops | bytes accessed | tf_op | source)
XLA Modules:
  0.0 325.0 jit_solution(2234047963984546768)
XLA Ops:
  7.2 1.0 copy-done
  8.2 5.2 %fusion.7 = f32[2304,256]{1,0:T(8,128)} fusion(bf16[1024,2304]{1,0:T(8,128)(2,1)} %param.12, bf16[1024,256]{1,0:T(8,128)(2,1)S(1)} %copy-done), kind=kOutput, calls=%fused_computation.27 | convolution fusion | flops 1207959552 | bytes 7602176 | tf_op jit(solution)/shard_map/dot_general | solution.py:46
  13.5 0.8 copy-done.3
  14.3 38.7 %all_gather.22 = bf16[2304,192]{1,0:T(8,128)(2,1)S(1)} all-gather(bf16[288,192]{1,0:T(8,128)(2,1)S(1)} %copy-done.3), channel_id=1, replica_groups=mesh['fs'=8,'tp'=4] {'fs'}, dimensions={0}, use_global_device_ids=true | all-gather | bytes 995328 | tf_op jit(solution)/shard_map/all_gather | solution.py:44
  53.0 4.8 %fusion = f32[192,256]{1,0:T(8,128)} fusion(bf16[1024,256]{1,0:T(8,128)(2,1)S(1)} %copy-done.10, bf16[1024,2304]{1,0:T(8,128)(2,1)} %param.15, bf16[2304,192]{1,0:T(8,128)(2,1)S(1)} %all_gather.22), kind=kOutput, calls=%fused_computation.4 | convolution fusion | flops 1006829568 | bytes 6324224 | tf_op jit(solution)/shard_map/dot_general | solution.py:55
  57.8 36.2 %reduce-scatter.2.cloned.1.call-done = f32[288,256]{1,0:T(8,128)} async-done(((f32[2304,256]{1,0:T(8,128)}), f32[288,256]{1,0:T(8,128)}) %reduce-scatter.2.cloned.1.call-update) | async-done | bytes 294928 | tf_op jit(solution)/shard_map/reduce_scatter | solution.py:45
  94.1 2.0 convolution_bitcast_fusion.2
  96.2 31.0 %all_gather.21 = f32[192,256]{1,0:T(8,128)S(1)} all-gather(f32[24,256]{1,0:T(8,128)S(1)} %copy-done.6), channel_id=1, replica_groups=mesh['fs'=8,'tp'=4] {'fs'}, dimensions={0}, use_global_device_ids=true | all-gather | bytes 221184 | tf_op jit(solution)/shard_map/all_gather | solution.py:61
  127.2 30.7 %all_gather.23 = f32[192,256]{1,0:T(8,128)S(1)} all-gather(f32[24,256]{1,0:T(8,128)S(1)} %copy-done.7), channel_id=1, replica_groups=mesh['fs'=8,'tp'=4] {'fs'}, dimensions={0}, use_global_device_ids=true | all-gather | bytes 221184 | tf_op jit(solution)/shard_map/all_gather | solution.py:62
  158.0 30.7 %all_gather.24 = f32[192,256]{1,0:T(8,128)S(1)} all-gather(f32[24,256]{1,0:T(8,128)S(1)} %copy-done.8), channel_id=1, replica_groups=mesh['fs'=8,'tp'=4] {'fs'}, dimensions={0}, use_global_device_ids=true | all-gather | bytes 221184 | tf_op jit(solution)/shard_map/all_gather | solution.py:63
  188.7 1.6 multiply_reduce_fusion
  190.3 1.6 multiply_reduce_fusion.1
  193.1 30.6 %all_gather.25 = f32[192,256]{1,0:T(8,128)S(1)} all-gather(f32[24,256]{1,0:T(8,128)S(1)} %copy-done.9), channel_id=1, replica_groups=mesh['fs'=8,'tp'=4] {'fs'}, dimensions={0}, use_global_device_ids=true | all-gather | bytes 221184 | tf_op jit(solution)/shard_map/all_gather | solution.py:64
  223.8 6.1 %psum.23 = f32[]{:T(128)} all-reduce(f32[]{:T(128)S(6)} %add.38), channel_id=1, replica_groups=mesh['fs'=8,'tp'=4] {'tp'}, use_global_device_ids=true, to_apply=%region_5.0 | all-reduce | flops 1 | bytes 8 | tf_op jit(solution)/shard_map/psum | solution.py:58
  230.6 1.1 fusion.1
  231.8 1.0 subtract_convert_fusion
  232.8 1.0 subtract_convert_fusion.1
  233.9 0.6 constant_dynamic-slice_fusion.2
  234.5 0.6 constant_dynamic-slice_fusion.3
  235.1 0.6 constant_dynamic-slice_fusion.1
  236.3 36.3 %all-gather.5.cloned.1.call-done = bf16[2304,256]{1,0:T(8,128)(2,1)} async-done(((bf16[288,256]{1,0:T(8,128)(2,1)}), bf16[2304,256]{1,0:T(8,128)(2,1)}) %all-gather.5.cloned.1.call-update) | async-done | bytes 1179664 | tf_op jit(solution)/shard_map/all_gather | solution.py:80
  272.6 42.4 %all-gather.3.cloned.1.call-done = bf16[2304,256]{1,0:T(8,128)(2,1)} async-done(((bf16[288,256]{1,0:T(8,128)(2,1)}), bf16[2304,256]{1,0:T(8,128)(2,1)}) %all-gather.3.cloned.1.call-update) | async-done | bytes 1179664 | tf_op jit(solution)/shard_map/all_gather | solution.py:79
  315.1 2.4 copy.24
  317.4 1.0 copy.25
  (30 shorter events, 0.9 us)
Async XLA Ops:
  7.2 1.0 copy-start
  7.2 86.9 %reduce-scatter.2.cloned.1.call-start = ((), (), s32[]{:S(2)}) async-start(), calls=%async_computation.1 | async-start | bytes 2654208 | tf_op jit(solution)/shard_map/reduce_scatter | solution.py:45
  13.4 0.9 copy-start.3
  13.4 39.6 %copy-start.10 = (bf16[1024,256]{1,0:T(8,128)(2,1)S(1)}, bf16[1024,256]{1,0:T(8,128)(2,1)}, u32[]{:S(2)}) copy-start(bf16[1024,256]{1,0:T(8,128)(2,1)} %param.14) | copy-start | bytes 1572868
  13.4 175.2 %all-reduce.3.cloned.1.call-start = ((), (), s32[]{:S(2)}) async-start(), calls=%async_computation.4 | async-start | bytes 786432 | tf_op jit(solution)/shard_map/psum | solution.py:57
  53.0 41.1 %copy-start.2 = (bf16[288,192]{1,0:T(8,128)(2,1)S(1)}, bf16[288,192]{1,0:T(8,128)(2,1)}, u32[]{:S(2)}) copy-start(bf16[288,192]{1,0:T(8,128)(2,1)} %param.16) | copy-start | bytes 331780
  53.0 43.2 %copy-start.6 = (f32[24,256]{1,0:T(8,128)S(1)}, f32[24,256]{1,0:T(8,128)}, u32[]{:S(2)}) copy-start(f32[24,256]{1,0:T(8,128)} %param.20) | copy-start | bytes 73732
  53.0 74.3 %copy-start.7 = (f32[24,256]{1,0:T(8,128)S(1)}, f32[24,256]{1,0:T(8,128)}, u32[]{:S(2)}) copy-start(f32[24,256]{1,0:T(8,128)} %param.21) | copy-start | bytes 73732
  53.0 105.0 %copy-start.8 = (f32[24,256]{1,0:T(8,128)S(1)}, f32[24,256]{1,0:T(8,128)}, u32[]{:S(2)}) copy-start(f32[24,256]{1,0:T(8,128)} %param.22) | copy-start | bytes 73732
  53.0 140.1 %copy-start.9 = (f32[24,256]{1,0:T(8,128)S(1)}, f32[24,256]{1,0:T(8,128)}, u32[]{:S(2)}) copy-start(f32[24,256]{1,0:T(8,128)} %param.23) | copy-start | bytes 73732
  57.8 173.9 %copy-start.4 = (f32[288,256]{1,0:T(8,128)S(1)}, f32[288,256]{1,0:T(8,128)}, u32[]{:S(2)}) copy-start(f32[288,256]{1,0:T(8,128)} %param.19) | copy-start | bytes 884740
  96.1 136.7 %copy-start.5 = (f32[288,256]{1,0:T(8,128)S(1)}, f32[288,256]{1,0:T(8,128)}, u32[]{:S(2)}) copy-start(f32[288,256]{1,0:T(8,128)} %param.18) | copy-start | bytes 884740
  96.1 176.5 %all-gather.5.cloned.1.call-start = ((), (), s32[]{:S(2)}) async-start(), calls=%async_computation.3 | async-start | bytes 1327104 | tf_op jit(solution)/shard_map/all_gather | solution.py:80
  232.8 82.3 %all-gather.3.cloned.1.call-start = ((), (), s32[]{:S(2)}) async-start(), calls=%async_computation.2 | async-start | bytes 1327104 | tf_op jit(solution)/shard_map/all_gather | solution.py:79
  272.6 44.8 %copy-start.1 = (bf16[2304,256]{1,0:T(8,128)(2,1)S(1)}, bf16[2304,256]{1,0:T(8,128)(2,1)}, u32[]{:S(2)}) copy-start(bf16[2304,256]{1,0:T(8,128)(2,1)} %all-gather.5.cloned.1.call-done) | copy-start | bytes 3538948
Sparse Core Ops, SparseCore 0:
  13.6 80.4 reduce-scatter.1
  98.0 71.2 all-reduce.2
  232.9 39.6 all-gather.4
  275.2 39.7 all-gather.2
where the time goes:
time: 325 us
  blocking collectives  168 us (52%)
  waiting for transfers between devices  115 us (35%)
  between operations  15.9 us (5%)
  matrix products  14 us (4%)
  local copies, waits for them, and re-layouts  7.69 us (2%)
  other arithmetic  4.31 us (1%)
    all_gather x1, waiting for transfers between devices, body(): lax.all_gather(copy_q, 'fs', axis=0, tiled=True)  42.4 us
    all_gather x1, blocking collectives, body(): lax.all_gather(out_factor, 'fs', axis=0, tiled=True)  38.7 us
    all_gather x1, waiting for transfers between devices, body(): lax.all_gather(copy_o, 'fs', axis=0, tiled=True)  36.3 us
    reduce_scatter x1, waiting for transfers between devices, body(): lax.psum_scatter(lax.dot_general(inputs, query_cot, contract_rows, prefer...  36.2 us
    all_gather x1, blocking collectives, body(): lax.all_gather(query_first, 'fs', axis=0, tiled=True)  31 us
    all_gather x1, blocking collectives, body(): lax.all_gather(query_second, 'fs', axis=0, tiled=True)  30.7 us
    all_gather x1, blocking collectives, body(): lax.all_gather(out_first, 'fs', axis=0, tiled=True)  30.7 us
    all_gather x1, blocking collectives, body(): lax.all_gather(out_second, 'fs', axis=0, tiled=True)  30.6 us
  transfers between devices with their start and end apart: 4, of which 3 were waited for; matrix products, arithmetic and copies ran while one was open for 3% of the time, Pallas kernels for 0%

commit v1 on v0

v1 whole, which is shorter than its diff:
```python
import functools
import math

import jax
import jax.numpy as jnp
from jax import lax
from jax.experimental import pallas as pl
from jax.experimental.pallas import tpu as pltpu
from jax.sharding import PartitionSpec as P

beta_first = 0.8
beta_second = 0.95
adam_eps = 1e-08
learn_rate = 0.05
norm_eps = 1e-06
contract_rows = (((0,), (0,)), ((), ()))
MESH = pl.DeviceIdType.MESH


def split_axis(n):
    ny = max(d for d in range(1, math.isqrt(n) + 1) if n % d == 0)
    return n // ny, ny


def kernel(
    n, tp, count,
    inputs, out_cot, query_factor, out_factor,
    query_cot, head_out, query_master, out_master,
    query_first, query_second, out_first, out_second,
    factors, masters, direction, first_q, second_q, first_o, second_o,
    xbuf, lows, terms, parts, got, squares, dirs, whole,
    local_sem, low_sem, fz_send, fz_recv, fy_send, fy_recv, fc_sem,
    mz_send, mz_recv, my_send, my_recv, rs_send, rs_recv, ss_sem, ag_send, ag_recv,
):
    nz, ny = split_axis(n)
    me, t = lax.axis_index("fs"), lax.axis_index("tp")
    z, y = me // ny, lax.rem(me, ny)
    core = lax.rem(t, 2)
    other = t + 1 - 2 * core
    total = n * tp
    mine = me * tp + t
    own = first_q.shape[0]

    @pl.when(core == 0)
    def _():
        pltpu.make_async_copy(query_factor, factors.at[core, me], local_sem.at[0]).start()
        pltpu.make_async_copy(inputs, xbuf, local_sem.at[1]).start()

    @pl.when(core == 1)
    def _():
        pltpu.make_async_copy(out_factor, factors.at[core, me], local_sem.at[0]).start()
        pltpu.make_async_copy(out_cot, xbuf, local_sem.at[1]).start()

    barrier = pltpu.get_barrier_semaphore()

    def greet(i, c):
        k = lax.rem(mine + i, total)
        pl.semaphore_signal(
            barrier, inc=1, device_id={"fs": k // tp, "tp": lax.rem(k, tp)}, device_id_type=MESH
        )
        return c

    lax.fori_loop(1, total, greet, 0)
    masters[me, 0] = query_master[...].astype(jnp.bfloat16)
    masters[me, 1] = out_master[...].astype(jnp.bfloat16)
    pl.semaphore_wait(barrier, total - 1)
    pltpu.make_async_copy(query_factor, factors.at[core, me], local_sem.at[0]).wait()

    def remote(src, dst, send, recv, f, tt=None):
        where = {"fs": f} if tt is None else {"fs": f, "tp": tt}
        return pltpu.make_async_remote_copy(
            src_ref=src, dst_ref=dst, send_sem=send, recv_sem=recv,
            device_id=where, device_id_type=MESH,
        )

    def along_z(buf, dz, send, recv):
        return remote(
            buf.at[me], buf.at[me], send.at[dz], recv.at[z], lax.rem(z + dz, nz) * ny + y
        )

    def from_z(buf, dz, send, recv):
        src = lax.rem(z + nz - dz, nz)
        piece = buf.at[src * ny + y]
        return remote(piece, piece, send.at[dz], recv.at[src], src * ny + y)

    def along_y(buf, zz, dy, send, recv):
        piece = buf.at[zz * ny + y]
        return remote(
            piece, piece, send.at[zz, dy], recv.at[zz, y], z * ny + lax.rem(y + dy, ny)
        )

    def from_y(buf, zz, dy, send, recv):
        src = lax.rem(y + ny - dy, ny)
        piece = buf.at[zz * ny + src]
        return remote(piece, piece, send.at[zz, dy], recv.at[zz, src], z * ny + src)

    def send_z(buf, send, recv):
        def go(dz, c):
            along_z(buf, dz, send, recv).start()
            return c
        lax.fori_loop(1, nz, go, 0)

    def send_y(buf, zz, send, recv):
        def go(dy, c):
            along_y(buf, zz, dy, send, recv).start()
            return c
        lax.fori_loop(1, ny, go, 0)

    def forward(buf, sz, rz, sy, ry):
        def go(dz, c):
            from_z(buf, dz, sz, rz).wait_recv()
            send_y(buf, lax.rem(z + nz - dz, nz), sy, ry)
            return c
        lax.fori_loop(1, nz, go, 0)

    def finish_recv_y(buf, sy, ry):
        def go(k, c):
            from_y(buf, k // (ny - 1), 1 + lax.rem(k, ny - 1), sy, ry).wait_recv()
            return c
        lax.fori_loop(0, nz * (ny - 1), go, 0)

    def finish_send(buf, sz, rz, sy, ry):
        def go_z(dz, c):
            along_z(buf, dz, sz, rz).wait_send()
            return c
        lax.fori_loop(1, nz, go_z, 0)

        def go_y(k, c):
            along_y(buf, k // (ny - 1), 1 + lax.rem(k, ny - 1), sy, ry).wait_send()
            return c
        lax.fori_loop(0, nz * (ny - 1), go_y, 0)

    fac = factors.at[core]
    f_sems = (fz_send, fz_recv, fy_send, fy_recv)
    send_z(fac, fz_send, fz_recv)
    send_y(fac, z, fy_send, fy_recv)
    forward(fac, *f_sems)
    pltpu.make_async_copy(inputs, xbuf, local_sem.at[1]).wait()
    finish_recv_y(fac, fy_send, fy_recv)
    share = remote(fac, fac, fc_sem.at[0], fc_sem.at[1], me, other)
    share.start()

    rank = factors.shape[-1]
    width = factors.shape[1] * factors.shape[2]
    if factors.shape[2] % 16 == 0:
        table = factors[core].reshape(width, rank)
    else:
        table = factors[core].astype(jnp.float32).reshape(width, rank).astype(jnp.bfloat16)
    tokens = xbuf.shape[0]
    tile = math.gcd(tokens, 256)

    def fold(i, c):
        at = pl.ds(pl.multiple_of(i * tile, tile), tile)
        lows[core, at, :] = jnp.dot(
            xbuf[at, :], table, preferred_element_type=jnp.float32
        ).astype(jnp.bfloat16)
        return c

    lax.fori_loop(0, tokens // tile, fold, 0)
    swap = remote(lows.at[core], lows.at[core], low_sem.at[0], low_sem.at[1], me, other)
    swap.start()
    swap.wait_recv()

    terms[0] = lax.dot_general(lows[0], query_cot[...], contract_rows, preferred_element_type=jnp.float32)
    terms[1] = lax.dot_general(lows[1], head_out[...], contract_rows, preferred_element_type=jnp.float32)
    for j in range(n):
        for w in range(2):
            parts[j, w] = terms[w, j * own:(j + 1) * own, :].astype(jnp.bfloat16)

    def scatter(i):
        f = lax.rem(me + i, n)
        return remote(parts.at[f], got.at[me], rs_send.at[f], rs_recv.at[me], f)

    def scattered(i):
        f = lax.rem(me + i, n)
        return remote(parts.at[f], got.at[f], rs_send.at[f], rs_recv.at[f], f)

    def each(make, act):
        def go(i, c):
            act(make(i))
            return c
        lax.fori_loop(1, n, go, 0)

    each(scatter, lambda d: d.start())
    m_sems = (mz_send, mz_recv, my_send, my_recv)
    send_z(masters, mz_send, mz_recv)
    send_y(masters, z, my_send, my_recv)
    each(scattered, lambda d: d.wait_recv())

    got[me] = parts[me]

    def add(j, c):
        return c + got[j].astype(jnp.float32)

    proj = lax.fori_loop(0, n, add, jnp.zeros(got.shape[1:], jnp.float32))
    sq = proj * proj
    row = jnp.sum(jnp.sum(sq, axis=0), axis=0, keepdims=True)
    squares[mine] = sum(row[:, k:k + 128] for k in range(0, row.shape[1], 128))

    def tell(i, c):
        k = lax.rem(mine + i, total)
        remote(
            squares.at[mine], squares.at[mine], ss_sem.at[0], ss_sem.at[1],
            k // tp, lax.rem(k, tp),
        ).start()
        return c

    lax.fori_loop(1, total, tell, 0)
    rest = squares.at[pl.ds(0, total - 1)]
    pltpu.make_async_copy(rest, rest, ss_sem.at[1]).wait()
    rms = jnp.sqrt(jnp.sum(squares[...]) / count + norm_eps)

    olds = ((query_first, query_second), (out_first, out_second))
    news = ((first_q, second_q), (first_o, second_o))
    for w in range(2):
        normed = proj[w] / rms
        first = beta_first * olds[w][0][...] + (1.0 - beta_first) * normed
        second = beta_second * olds[w][1][...] + (1.0 - beta_second) * normed * normed
        news[w][0][...] = first
        news[w][1][...] = second
        dirs[me, w] = (first / (jnp.sqrt(second) + adam_eps)).astype(jnp.bfloat16)

    def spread(i):
        f = lax.rem(me + i, n)
        return remote(dirs.at[me], dirs.at[me], ag_send.at[f], ag_recv.at[me], f)

    def arrived(i):
        f = lax.rem(me + i, n)
        return remote(dirs.at[f], dirs.at[f], ag_send.at[f], ag_recv.at[f], f)

    each(spread, lambda d: d.start())
    forward(masters, *m_sems)
    each(arrived, lambda d: d.wait_recv())
    for w in range(2):
        for j in range(n):
            whole[j * own:(j + 1) * own, :] = dirs[j, w].astype(jnp.float32)
        direction[w] = whole[...].astype(jnp.bfloat16)

    finish_recv_y(masters, my_send, my_recv)
    back = factors.at[1 - core]
    remote(back, back, fc_sem.at[0], fc_sem.at[1], me, other).wait_recv()
    share.wait_send()
    swap.wait_send()
    finish_send(fac, *f_sems)
    finish_send(masters, *m_sems)
    each(scatter, lambda d: d.wait_send())
    each(spread, lambda d: d.wait_send())
    pltpu.make_async_copy(rest, rest, ss_sem.at[0]).wait()


def exchange(n, tp, inputs, out_cot, query_factor, out_factor, query_cot, head_out,
             query_master, out_master, *moments):
    rows, rank = query_factor.shape
    cols = query_cot.shape[1]
    own = moments[0].shape[0]
    tokens, width = inputs.shape
    nz, ny = split_axis(n)
    vmem = pl.BlockSpec(memory_space=pltpu.VMEM)
    anyspace = pl.BlockSpec(memory_space=pl.ANY)
    dma = pltpu.SemaphoreType.DMA
    bf, f32 = jnp.bfloat16, jnp.float32
    shape = jax.ShapeDtypeStruct
    return pl.pallas_call(
        functools.partial(kernel, n, tp, 2.0 * rank * cols * tp),
        out_shape=(
            shape((2, n, rows, rank), bf),
            shape((n, 2, rows, cols), bf),
            shape((2, rank, cols), bf),
            *(shape((own, cols), f32) for _ in range(4)),
        ),
        in_specs=[anyspace] * 4 + [vmem] * 8,
        out_specs=(vmem,) * 7,
        scratch_shapes=[
            pltpu.VMEM((tokens, width), bf),
            pltpu.VMEM((2, tokens, rank), bf),
            pltpu.VMEM((2, rank, cols), f32),
            pltpu.VMEM((n, 2, own, cols), bf),
            pltpu.VMEM((n, 2, own, cols), bf),
            pltpu.VMEM((n * tp, 1, 128), f32),
            pltpu.VMEM((n, 2, own, cols), bf),
            pltpu.VMEM((rank, cols), f32),
            dma((2,)), dma((2,)),
            dma((nz,)), dma((nz,)), dma((nz, ny)), dma((nz, ny)), dma((2,)),
            dma((nz,)), dma((nz,)), dma((nz, ny)), dma((nz, ny)),
            dma((n,)), dma((n,)), dma((2,)), dma((n,)), dma((n,)),
        ],
        compiler_params=pltpu.CompilerParams(
            collective_id=0, has_side_effects=True, vmem_limit_bytes=56 * 1024 * 1024
        ),
    )(inputs, out_cot, query_factor, out_factor, query_cot, head_out,
      query_master, out_master, *moments)


def body(
    n, tp, inputs, query_cot, head_out, out_cot, query_factor, out_factor,
    query_master, out_master, query_first, query_second, out_first, out_second,
):
    factors, masters, direction, first_q, second_q, first_o, second_o = exchange(
        n, tp, inputs, out_cot, query_factor, out_factor, query_cot, head_out,
        query_master, out_master, query_first, query_second, out_first, out_second,
    )
    rank = query_factor.shape[1]
    cols = query_cot.shape[1]

    def dot(a, b):
        return jnp.dot(a, b, preferred_element_type=jnp.float32)

    query_step = dot(query_factor, direction[0])
    out_step = dot(out_factor, direction[1])
    copies = []
    for w in range(2):
        step = dot(factors[w].reshape(-1, rank), direction[w])
        master = masters[:, w].reshape(-1, cols).astype(jnp.float32)
        copies.append((master - learn_rate * step).astype(jnp.bfloat16))
    return (query_step, out_step, *copies, first_q, second_q, first_o, second_o)


def solution(mesh):
    rows, both = P("fs", None), P("fs", "tp")
    return jax.shard_map(
        functools.partial(body, mesh.shape["fs"], mesh.shape["tp"]),
        mesh=mesh,
        in_specs=(rows, both, both, rows, rows, rows) + (both,) * 6,
        out_specs=(both, both, P(None, "tp"), P(None, "tp")) + (both,) * 4,
        check_vma=False,
    )
```

time: 325 us -> 98.2 us (0.30)
  blocking collectives: 168 us -> 0 us
  waiting for transfers between devices: 115 us -> 0 us
  Pallas kernels: 0 us -> 86.8 us
  between operations: 15.9 us -> 0.68 us
  matrix products: 14 us -> 4.74 us
  other arithmetic: 4.31 us -> 0 us
    all_gather x5 -> x0, blocking collectives: 162 us -> none  [the longest x1 38.7 us: body(): lax.all_gather(out_factor, 'fs', axis=0, tiled=True)]
    pallas_call x0 -> x1, Pallas kernels: none -> 86.8 us  [exchange(): pl.pallas_call(functools.partial(kernel, n, tp, 2.0 * rank * cols * tp),...]
    all_gather x2 -> x0, waiting for transfers between devices: 78.7 us -> none  [the longest x1 42.4 us: body(): lax.all_gather(copy_q, 'fs', axis=0, tiled=True)]
    reduce_scatter x1 -> x0, waiting for transfers between devices: 36.2 us -> none  [body(): lax.psum_scatter(lax.dot_general(inputs, query_cot, contract_rows, prefer...]
    dot_general x5 -> x4, matrix products: 14 us -> 4.74 us  [dot(): return jnp.dot(a, b, preferred_element_type=jnp.float32)]
    psum x1 -> x0, blocking collectives: 6.14 us -> none  [body(): lax.psum(jnp.sum(whole_q * whole_q) + jnp.sum(whole_o * whole_o), 'tp')]
  transfers between devices with their start and end apart: 4 -> 0, of which waited for: 3 -> 0; matrix products, arithmetic and copies ran while one was open for 3% -> 0% of each run, Pallas kernels for 0% -> 0%
where the time goes in v1:
time: 98.2 us; the launch traced here: 98 us
  Pallas kernels  86.8 us (88%)
  local copies, waits for them, and re-layouts  5.74 us (6%)
  matrix products  4.74 us (5%)
    pallas_call x1, Pallas kernels, exchange(): pl.pallas_call(functools.partial(kernel, n, tp, 2.0 * rank * cols * tp),...  86.8 us
    dot_general x4, matrix products, dot(): return jnp.dot(a, b, preferred_element_type=jnp.float32)  4.74 us
    unnamed x20, local copies, waits for them, and re-layouts  3.65 us

profile of v1, /device:TPU:0, one launch (start us, length us, event | category | flops | bytes accessed | tf_op | source)
XLA Modules:
  0.0 98.0 jit_solution(8733579306314489993)
XLA Ops:
  0.6 86.8 %shard_map.179 = (bf16[2,8,288,192]{3,2,1,0:T(8,128)(2,1)}, bf16[8,2,288,256]{3,2,1,0:T(8,128)(2,1)}, bf16[2,192,256]{2,1,0:T(8,128)(2,1)}, f32[24,256]{1,0:T(8,...) custom-call(bf16[1024,2304]{1,0:T(8,128)(2,1)} %inputs.1, bf16[1024,2304]{1,0:T(8,128)(2,1)} %out_cot.1, ...), custom_call_target="tpu_custom_call" | custom-call | tf_op jit(solution)/shard_map/pallas_call | solution.py:263
  87.5 0.0 copy-start
  87.5 1.9 %fusion.13 = (bf16[1,8,288,192]{3,2,1,0:T(8,128)(2,1)S(1)}, bf16[1,8,288,192]{3,2,1,0:T(8,128)(2,1)S(1)}) fusion(bf16[2,8,288,192]{3,2,1,0:T(8,128)(2,1)} %get-tuple-element.17), kind=kLoop, calls=%fused_computation.17 | loop fusion | bytes 3538944 | tf_op jit(solution)/shard_map/slice | solution.py:312
  89.4 0.4 copy-done
  89.9 0.0 copy-start.1
  89.9 0.2 fusion.12
  90.0 0.8 copy-done.1
  90.8 1.5 %fusion.3 = bf16[2304,256]{1,0:T(8,128)(2,1)} fusion(bf16[2304,192]{1,0:T(8,128)(2,1)S(1)} %bitcast.25, bf16[2304,256]{1,0:T(8,128)(2,1)S(1)} %bitcast.27, bf16[2,192,256]{2,1,0:T(8,128)(2,1)S(1)} %copy-done.1), kind=kOutput, calls=%fused_computation.5 | convolution fusion | flops 228851712 | bytes 3637248 | tf_op jit(solution)/shard_map/dot_general | solution.py:306
  92.3 0.0 copy-start.2
  92.3 0.0 copy-start.3
  92.3 0.0 copy-start.7
  92.3 1.5 %fusion.2 = bf16[2304,256]{1,0:T(8,128)(2,1)} fusion(bf16[2304,192]{1,0:T(8,128)(2,1)S(1)} %bitcast.24, bf16[2304,256]{1,0:T(8,128)(2,1)S(1)} %bitcast.26, bf16[2,192,256]{2,1,0:T(8,128)(2,1)S(1)} %copy-done.1), kind=kOutput, calls=%fused_computation.4 | convolution fusion | flops 228851712 | bytes 3637248 | tf_op jit(solution)/shard_map/dot_general | solution.py:306
  93.7 0.0 copy-done.2
  93.7 0.9 convolution_bitcast_fusion
  94.6 0.0 copy-done.3
  94.6 0.9 convolution_bitcast_fusion.1
  95.5 0.0 copy-done.7
  95.5 0.6 copy.24
  96.2 0.0 copy-done.6
  96.2 0.6 copy.25
  96.8 0.0 copy-done.5
  96.8 0.6 copy.26
  97.4 0.0 copy-done.4
  97.4 0.6 copy.27
  (3 shorter events, 0.0 us)
Async XLA Ops:
  87.5 2.4 %copy-start = (bf16[8,2,288,256]{3,2,1,0:T(8,128)(2,1)S(1)}, bf16[8,2,288,256]{3,2,1,0:T(8,128)(2,1)}, u32[]{:S(2)}) copy-start(bf16[8,2,288,256]{3,2,1,0:T(8,128)(2,1)} %get-tuple-element.16) | copy-start | bytes 7077892
  89.9 0.9 copy-start.1
  92.3 1.5 %copy-start.2 = (bf16[288,192]{1,0:T(8,128)(2,1)S(1)}, bf16[288,192]{1,0:T(8,128)(2,1)}, u32[]{:S(2)}) copy-start(bf16[288,192]{1,0:T(8,128)(2,1)} %out_factor.1) | copy-start | bytes 331780
  92.3 2.4 %copy-start.3 = (bf16[288,192]{1,0:T(8,128)(2,1)S(1)}, bf16[288,192]{1,0:T(8,128)(2,1)}, u32[]{:S(2)}) copy-start(bf16[288,192]{1,0:T(8,128)(2,1)} %query_factor.1) | copy-start | bytes 331780
  92.3 3.3 %copy-start.7 = (f32[24,256]{1,0:T(8,128)S(1)}, f32[24,256]{1,0:T(8,128)}, u32[]{:S(2)}) copy-start(f32[24,256]{1,0:T(8,128)} %get-tuple-element.38) | copy-start | bytes 73732
  92.3 3.9 %copy-start.6 = (f32[24,256]{1,0:T(8,128)S(1)}, f32[24,256]{1,0:T(8,128)}, u32[]{:S(2)}) copy-start(f32[24,256]{1,0:T(8,128)} %get-tuple-element.39) | copy-start | bytes 73732
  93.7 3.0 %copy-start.5 = (f32[24,256]{1,0:T(8,128)S(1)}, f32[24,256]{1,0:T(8,128)}, u32[]{:S(2)}) copy-start(f32[24,256]{1,0:T(8,128)} %get-tuple-element.40) | copy-start | bytes 73732
  93.7 3.6 %copy-start.4 = (f32[24,256]{1,0:T(8,128)S(1)}, f32[24,256]{1,0:T(8,128)}, u32[]{:S(2)}) copy-start(f32[24,256]{1,0:T(8,128)} %get-tuple-element.41) | copy-start | bytes 73732

commit v2 on v1

v2 whole, which is shorter than its diff:
```python
import functools
import math

import jax
import jax.numpy as jnp
from jax import lax
from jax.experimental import pallas as pl
from jax.experimental.pallas import tpu as pltpu
from jax.sharding import PartitionSpec as P

beta_first = 0.8
beta_second = 0.95
adam_eps = 1e-08
learn_rate = 0.05
norm_eps = 1e-06
contract_rows = (((0,), (0,)), ((), ()))
MESH = pl.DeviceIdType.MESH


def shares_of(tp, rows):
    return tp // 2 if rows % (tp // 2 * 16) == 0 else 1


def split_axis(n):
    ny = max(d for d in range(1, math.isqrt(n) + 1) if n % d == 0)
    return n // ny, ny


def moments(normed, first, second):
    first_new = beta_first * first + (1.0 - beta_first) * normed
    second_new = beta_second * second + (1.0 - beta_second) * normed * normed
    return first_new, second_new


def finish(
    factors, masters, direction, normed, query_first, query_second, out_first, out_second,
    query_step, out_step, query_copy, out_copy, first_q, second_q, first_o, second_o,
):
    j = pl.program_id(0)

    @pl.when(j == 0)
    def _():
        first_q[...], second_q[...] = moments(normed[0], query_first[...], query_second[...])
        first_o[...], second_o[...] = moments(normed[1], out_first[...], out_second[...])

    for w, (step_out, copy) in enumerate(((query_step, query_copy), (out_step, out_copy))):
        step = jnp.dot(factors[w, 0], direction[w], preferred_element_type=jnp.float32)
        copy[...] = (masters[0, w].astype(jnp.float32) - learn_rate * step).astype(copy.dtype)

        @pl.when(j == lax.axis_index("fs"))
        def _():
            step_out[...] = step


def kernel(
    n, tp, count,
    inputs, out_cot, query_factor, out_factor,
    query_cot, head_out, query_master, out_master,
    query_first, query_second, out_first, out_second,
    factors, masters, direction, normed_out,
    xbuf, lows, terms, parts, got, squares, dirs, whole,
    local_sem, low_sem, fu_send, fd_send, fz_recv, fy_send, fy_recv, fx_send, fx_recv, fc_sem,
    mu_send, md_send, mz_recv, my_send, my_recv, rs_send, rs_recv, ss_sem, ag_send, ag_recv,
):
    nz, ny = split_axis(n)
    me, t = lax.axis_index("fs"), lax.axis_index("tp")
    z, y = me // ny, lax.rem(me, ny)
    core = lax.rem(t, 2)
    other = t + 1 - 2 * core
    total = n * tp
    mine = me * tp + t
    own = query_first.shape[0]

    def own_factor(source):
        return pltpu.make_async_copy(source, factors.at[core, me], local_sem.at[0])

    @pl.when(core == 0)
    def _():
        own_factor(query_factor).start()
        pltpu.make_async_copy(inputs, xbuf, local_sem.at[1]).start()

    @pl.when(core == 1)
    def _():
        own_factor(out_factor).start()
        pltpu.make_async_copy(out_cot, xbuf, local_sem.at[1]).start()

    barrier = pltpu.get_barrier_semaphore()

    def greet(i, c):
        k = lax.rem(mine + i, total)
        pl.semaphore_signal(
            barrier, inc=1, device_id={"fs": k // tp, "tp": lax.rem(k, tp)}, device_id_type=MESH
        )
        return c

    lax.fori_loop(1, total, greet, 0)
    masters[me, 0] = query_master[...].astype(jnp.bfloat16)
    masters[me, 1] = out_master[...].astype(jnp.bfloat16)
    pl.semaphore_wait(barrier, total - 1)
    own_factor(query_factor).wait()

    def remote(src, dst, send, recv, f, tt=None):
        where = {"fs": f} if tt is None else {"fs": f, "tp": tt}
        return pltpu.make_async_remote_copy(
            src_ref=src, dst_ref=dst, send_sem=send, recv_sem=recv,
            device_id=where, device_id_type=MESH,
        )

    def up(piece, zz, sems):
        return remote(piece(zz, y), piece(zz, y), sems[0].at[zz], sems[2].at[zz], me + ny)

    def down(piece, zz, sems):
        return remote(piece(zz, y), piece(zz, y), sems[1].at[zz], sems[2].at[zz], me - ny)

    def along_y(piece, zz, dy, sems):
        return remote(
            piece(zz, y), piece(zz, y), sems[3].at[zz, dy], sems[4].at[zz, y],
            z * ny + lax.rem(y + dy, ny),
        )

    def from_y(piece, zz, dy, sems):
        src = lax.rem(y + ny - dy, ny)
        return remote(
            piece(zz, src), piece(zz, src), sems[3].at[zz, dy], sems[4].at[zz, src], z * ny + src
        )

    def loop(low, high, act):
        def go(i, c):
            act(i)
            return c
        lax.fori_loop(low, high, go, 0)

    def hops(piece, low, high, sems, extra=None):
        def pass_on(zz, come, up_too, down_too):
            @pl.when(come)
            def _():
                @pl.when(zz != z)
                def _():
                    up(piece, zz, sems).wait_recv()

                @pl.when(up_too)
                def _():
                    up(piece, zz, sems).start()

                @pl.when(down_too)
                def _():
                    down(piece, zz, sems).start()

                loop(1, ny, lambda dy: along_y(piece, zz, dy, sems).start())
                if extra is not None:
                    extra(zz, y)

        def step(k):
            pass_on(z - k, z >= k, z < nz - 1, (k == 0) & (z > 0))
            pass_on(z + k, (k > 0) & (z + k < nz), z < 0, z > 0)

        loop(low, high, step)

    def all_y(act):
        loop(0, nz * (ny - 1), lambda k: act(k // (ny - 1), 1 + lax.rem(k, ny - 1)))

    def sent(piece, sems):
        @pl.when(z < nz - 1)
        def _():
            loop(0, z + 1, lambda zz: up(piece, zz, sems).wait_send())

        @pl.when(z > 0)
        def _():
            loop(z, nz, lambda zz: down(piece, zz, sems).wait_send())

        all_y(lambda zz, dy: along_y(piece, zz, dy, sems).wait_send())

    shares = factors.shape[2]
    part = lax.rem(t // 2, shares)

    def f_piece(zz, yy):
        return factors.at[core, zz * ny + yy, part]

    def m_piece(zz, yy):
        return masters.at[zz * ny + yy]

    def over_x(zz, yy, dx):
        block = zz * ny + yy
        piece = factors.at[core, block, part]
        return remote(
            piece, piece, fx_send.at[block, dx], fx_recv.at[block, part],
            me, 2 * lax.rem(part + dx, shares) + core,
        )

    def from_x(zz, yy, dx):
        block = zz * ny + yy
        src = lax.rem(part + shares - dx, shares)
        piece = factors.at[core, block, src]
        return remote(
            piece, piece, fx_send.at[block, dx], fx_recv.at[block, src], me, 2 * src + core
        )

    def send_x(zz, yy):
        @pl.when(zz * ny + yy != me)
        def _():
            for dx in range(1, shares):
                over_x(zz, yy, dx).start()

    f_sems = (fu_send, fd_send, fz_recv, fy_send, fy_recv)
    m_sems = (mu_send, md_send, mz_recv, my_send, my_recv)
    hops(f_piece, 0, nz, f_sems, send_x)
    hops(m_piece, 0, 1, m_sems)
    pltpu.make_async_copy(inputs, xbuf, local_sem.at[1]).wait()

    def take_y(zz, dy):
        from_y(f_piece, zz, dy, f_sems).wait_recv()
        send_x(zz, lax.rem(y + ny - dy, ny))

    all_y(take_y)

    def others(act):
        for dx in range(1, shares):
            loop(1, n, lambda i: act(lax.rem(me + i, n) // ny, lax.rem(me + i, ny), dx))

    others(lambda zz, yy, dx: from_x(zz, yy, dx).wait_recv())
    fac = factors.at[core]
    share = remote(fac, fac, fc_sem.at[0], fc_sem.at[1], me, other)
    share.start()

    rank = factors.shape[-1]
    width = inputs.shape[1]
    if factors.shape[3] % 16 == 0:
        table = factors[core].reshape(width, rank)
    else:
        table = factors[core].astype(jnp.float32).reshape(width, rank).astype(jnp.bfloat16)
    tokens = xbuf.shape[0]
    tile = math.gcd(tokens, 256)

    def fold(i, c):
        at = pl.ds(pl.multiple_of(i * tile, tile), tile)
        lows[core, at, :] = jnp.dot(
            xbuf[at, :], table, preferred_element_type=jnp.float32
        ).astype(jnp.bfloat16)
        return c

    lax.fori_loop(0, tokens // tile, fold, 0)
    swap = remote(lows.at[core], lows.at[core], low_sem.at[0], low_sem.at[1], me, other)
    swap.start()
    swap.wait_recv()

    terms[0] = lax.dot_general(lows[0], query_cot[...], contract_rows, preferred_element_type=jnp.float32)
    terms[1] = lax.dot_general(lows[1], head_out[...], contract_rows, preferred_element_type=jnp.float32)
    for j in range(n):
        for w in range(2):
            parts[j, w] = terms[w, j * own:(j + 1) * own, :].astype(jnp.bfloat16)

    def scatter(i):
        f = lax.rem(me + i, n)
        return remote(parts.at[f], got.at[me], rs_send.at[f], rs_recv.at[me], f)

    def scattered(i):
        f = lax.rem(me + i, n)
        return remote(parts.at[f], got.at[f], rs_send.at[f], rs_recv.at[f], f)

    def each(make, act):
        def go(i, c):
            act(make(i))
            return c
        lax.fori_loop(1, n, go, 0)

    each(scatter, lambda d: d.start())
    hops(m_piece, 1, 2, m_sems)
    each(scattered, lambda d: d.wait_recv())

    got[me] = parts[me]

    def add(j, c):
        return c + got[j].astype(jnp.float32)

    proj = lax.fori_loop(0, n, add, jnp.zeros(got.shape[1:], jnp.float32))
    sq = proj * proj
    row = jnp.sum(jnp.sum(sq, axis=0), axis=0, keepdims=True)
    squares[mine] = sum(row[:, k:k + 128] for k in range(0, row.shape[1], 128))

    def tell(i, c):
        k = lax.rem(mine + i, total)
        remote(
            squares.at[mine], squares.at[mine], ss_sem.at[0], ss_sem.at[1],
            k // tp, lax.rem(k, tp),
        ).start()
        return c

    lax.fori_loop(1, total, tell, 0)
    rest = squares.at[pl.ds(0, total - 1)]
    pltpu.make_async_copy(rest, rest, ss_sem.at[1]).wait()
    rms = jnp.sqrt(jnp.sum(squares[...]) / count + norm_eps)

    olds = ((query_first, query_second), (out_first, out_second))
    for w in range(2):
        normed = proj[w] / rms
        normed_out[w] = normed
        first, second = moments(normed, olds[w][0][...], olds[w][1][...])
        dirs[me, w] = (first / (jnp.sqrt(second) + adam_eps)).astype(jnp.bfloat16)

    def spread(i):
        f = lax.rem(me + i, n)
        return remote(dirs.at[me], dirs.at[me], ag_send.at[f], ag_recv.at[me], f)

    def arrived(i):
        f = lax.rem(me + i, n)
        return remote(dirs.at[f], dirs.at[f], ag_send.at[f], ag_recv.at[f], f)

    each(spread, lambda d: d.start())
    hops(m_piece, 2, nz, m_sems)
    each(arrived, lambda d: d.wait_recv())
    for w in range(2):
        for j in range(n):
            whole[j * own:(j + 1) * own, :] = dirs[j, w].astype(jnp.float32)
        direction[w] = whole[...].astype(jnp.bfloat16)

    all_y(lambda zz, dy: from_y(m_piece, zz, dy, m_sems).wait_recv())
    back = factors.at[1 - core]
    remote(back, back, fc_sem.at[0], fc_sem.at[1], me, other).wait_recv()
    share.wait_send()
    swap.wait_send()
    sent(f_piece, f_sems)
    sent(m_piece, m_sems)
    others(lambda zz, yy, dx: over_x(zz, yy, dx).wait_send())
    each(scatter, lambda d: d.wait_send())
    each(spread, lambda d: d.wait_send())
    pltpu.make_async_copy(rest, rest, ss_sem.at[0]).wait()


def exchange(n, tp, inputs, out_cot, query_factor, out_factor, query_cot, head_out,
             query_master, out_master, *olds):
    rows = query_master.shape[0]
    rank = query_factor.shape[-1]
    cols = query_cot.shape[1]
    own = olds[0].shape[0]
    tokens, width = inputs.shape
    nz, ny = split_axis(n)
    vmem = pl.BlockSpec(memory_space=pltpu.VMEM)
    anyspace = pl.BlockSpec(memory_space=pl.ANY)
    dma = pltpu.SemaphoreType.DMA
    bf, f32 = jnp.bfloat16, jnp.float32
    shares = shares_of(tp, rows)
    gather = (dma((nz,)), dma((nz,)), dma((nz,)), dma((nz, ny)), dma((nz, ny)))
    shape = jax.ShapeDtypeStruct
    return pl.pallas_call(
        functools.partial(kernel, n, tp, 2.0 * rank * cols * tp),
        out_shape=(
            shape((2, n, shares, rows // shares, rank), bf),
            shape((n, 2, rows, cols), bf),
            shape((2, rank, cols), bf),
            shape((2, own, cols), f32),
        ),
        in_specs=[anyspace] * 4 + [vmem] * 8,
        out_specs=(vmem,) * 4,
        scratch_shapes=[
            pltpu.VMEM((tokens, width), bf),
            pltpu.VMEM((2, tokens, rank), bf),
            pltpu.VMEM((2, rank, cols), f32),
            pltpu.VMEM((n, 2, own, cols), bf),
            pltpu.VMEM((n, 2, own, cols), bf),
            pltpu.VMEM((n * tp, 1, 128), f32),
            pltpu.VMEM((n, 2, own, cols), bf),
            pltpu.VMEM((rank, cols), f32),
            dma((2,)), dma((2,)),
            *gather, dma((n, shares)), dma((n, shares)), dma((2,)),
            *gather,
            dma((n,)), dma((n,)), dma((2,)), dma((n,)), dma((n,)),
        ],
        compiler_params=pltpu.CompilerParams(
            collective_id=0, has_side_effects=True, vmem_limit_bytes=56 * 1024 * 1024
        ),
    )(inputs, out_cot, query_factor, out_factor, query_cot, head_out,
      query_master, out_master, *olds)


def body(
    n, tp, inputs, query_cot, head_out, out_cot, query_factor, out_factor,
    query_master, out_master, query_first, query_second, out_first, out_second,
):
    rows = query_factor.shape[0]
    shares = shares_of(tp, rows)

    def split(factor):
        return factor.reshape(shares, rows // shares, -1)

    factors, masters, direction, normed = exchange(
        n, tp, inputs, out_cot, split(query_factor), split(out_factor), query_cot, head_out,
        query_master, out_master, query_first, query_second, out_first, out_second,
    )
    rank = query_factor.shape[1]
    own, cols = query_first.shape
    f32, bf = jnp.float32, jnp.bfloat16
    factors = factors.reshape(2, n, rows, rank)
    shape = jax.ShapeDtypeStruct

    def fixed(*dims):
        return pl.BlockSpec(dims, lambda j: (0,) * len(dims))

    block = pl.BlockSpec((rows, cols), lambda j: (j, 0))
    return pl.pallas_call(
        finish,
        grid=(n,),
        in_specs=[
            pl.BlockSpec((2, 1, rows, rank), lambda j: (0, j, 0, 0)),
            pl.BlockSpec((1, 2, rows, cols), lambda j: (j, 0, 0, 0)),
            fixed(2, rank, cols),
            fixed(2, own, cols),
        ] + [fixed(own, cols)] * 4,
        out_specs=[fixed(rows, cols)] * 2 + [block] * 2 + [fixed(own, cols)] * 4,
        out_shape=[shape((rows, cols), f32)] * 2
        + [shape((n * rows, cols), bf)] * 2
        + [shape((own, cols), f32)] * 4,
    )(factors, masters, direction, normed, query_first, query_second, out_first, out_second)


def solution(mesh):
    rows, both = P("fs", None), P("fs", "tp")
    return jax.shard_map(
        functools.partial(body, mesh.shape["fs"], mesh.shape["tp"]),
        mesh=mesh,
        in_specs=(rows, both, both, rows, rows, rows) + (both,) * 6,
        out_specs=(both, both, P(None, "tp"), P(None, "tp")) + (both,) * 4,
        check_vma=False,
    )
```

time: 98.2 us -> 75.7 us (0.77)
  Pallas kernels: 86.8 us -> 74.7 us
  local copies, waits for them, and re-layouts: 5.74 us -> 0 us
  matrix products: 4.74 us -> 0 us
    pallas_call x1, Pallas kernels: 86.8 us -> 66.6 us  [exchange(): pl.pallas_call(functools.partial(kernel, n, tp, 2.0 * rank * cols * tp),...]
    pallas_call x0 -> x1, Pallas kernels: none -> 8.11 us  [body(): pl.pallas_call(finish, grid=(n,), in_specs=[pl.BlockSpec((2, 1, rows, ran...]
    dot_general x4 -> x0, matrix products: 4.74 us -> none  [dot(): return jnp.dot(a, b, preferred_element_type=jnp.float32)]
    unnamed x20 -> x0, local copies, waits for them, and re-layouts: 3.65 us -> none
    slice x2 -> x0, local copies, waits for them, and re-layouts: 2.09 us -> none  [the longest x1 1.93 us: body(): step = dot(factors[w].reshape(-1, rank), direction[w])]
where the time goes in v2:
time: 75.7 us; the launch traced here: 75.4 us
  Pallas kernels  74.7 us (99%)
    pallas_call x1, Pallas kernels, exchange(): pl.pallas_call(functools.partial(kernel, n, tp, 2.0 * rank * cols * tp),...  66.6 us
    pallas_call x1, Pallas kernels, body(): pl.pallas_call(finish, grid=(n,), in_specs=[pl.BlockSpec((2, 1, rows, ran...  8.11 us

profile of v2, /device:TPU:0, one launch (start us, length us, event | category | flops | bytes accessed | tf_op | source)
XLA Modules:
  0.0 75.4 jit_solution(3821707847194434104)
XLA Ops:
  0.6 66.6 %shard_map.179 = (bf16[2,8,2,144,192]{4,3,2,1,0:T(8,128)(2,1)}, bf16[8,2,288,256]{3,2,1,0:T(8,128)(2,1)}, bf16[2,192,256]{2,1,0:T(8,128)(2,1)}, f32[2,24,256]{2,1,0:T(8,128)}) custom-call(bf16[1024,2304]{1,0:T(8,128)(2,1)} %inputs.1, bf16[1024,2304]{1,0:T(8,128)(2,1)} %out_cot.1, bf16[2,144,192]{2,1,0:T(8,128)(2,1)} %bitcast.4, ...), custom_call_target="tpu_custom_call" | custom-call | tf_op jit(solution)/shard_map/pallas_call | solution.py:344
  67.3 8.1 %shard_map.180 = (f32[288,256]{1,0:T(8,128)}, f32[288,256]{1,0:T(8,128)}, bf16[2304,256]{1,0:T(8,128)(2,1)}, bf16[2304,256]{1,0:T(8,128)(2,1)}, f32[24,256]{1,0:...) custom-call(bf16[2,8,288,192]{3,2,1,0:T(8,128)(2,1)} %bitcast.3, ...), custom_call_target="tpu_custom_call" | custom-call | tf_op jit(solution)/shard_map/pallas_call | solution.py:399

commit v3 on v2

--- a/solution.py
+++ b/solution.py
@@ -43,13 +43,21 @@
         first_q[...], second_q[...] = moments(normed[0], query_first[...], query_second[...])
         first_o[...], second_o[...] = moments(normed[1], out_first[...], out_second[...])
 
-    for w, (step_out, copy) in enumerate(((query_step, query_copy), (out_step, out_copy))):
-        step = jnp.dot(factors[w, 0], direction[w], preferred_element_type=jnp.float32)
-        copy[...] = (masters[0, w].astype(jnp.float32) - learn_rate * step).astype(copy.dtype)
-
-        @pl.when(j == lax.axis_index("fs"))
-        def _():
-            step_out[...] = step
+    me = lax.axis_index("fs")
+    blocks, rows = factors.shape[1:3]
+
+    def one(i, c):
+        at = pl.ds(pl.multiple_of(i * rows, 8), rows)
+        for w, (step_out, copy) in enumerate(((query_step, query_copy), (out_step, out_copy))):
+            step = jnp.dot(factors[w, i], direction[w], preferred_element_type=jnp.float32)
+            copy[at, :] = (masters[w, i].astype(jnp.float32) - learn_rate * step).astype(copy.dtype)
+
+            @pl.when(j * blocks + i == me)
+            def _():
+                step_out[...] = step
+        return c
+
+    lax.fori_loop(0, blocks, one, 0)
 
 
 def kernel(
@@ -59,7 +67,7 @@
     query_first, query_second, out_first, out_second,
     factors, masters, direction, normed_out,
     xbuf, lows, terms, parts, got, squares, dirs, whole,
-    local_sem, low_sem, fu_send, fd_send, fz_recv, fy_send, fy_recv, fx_send, fx_recv, fc_sem,
+    local_sem, low_sem, fz_send, fz_recv, fy_send, fy_recv, fx_send, fx_recv, fc_sem,
     mu_send, md_send, mz_recv, my_send, my_recv, rs_send, rs_recv, ss_sem, ag_send, ag_recv,
 ):
     nz, ny = split_axis(n)
@@ -86,17 +94,30 @@
 
     barrier = pltpu.get_barrier_semaphore()
 
-    def greet(i, c):
-        k = lax.rem(mine + i, total)
+    def greet(f, tt):
         pl.semaphore_signal(
-            barrier, inc=1, device_id={"fs": k // tp, "tp": lax.rem(k, tp)}, device_id_type=MESH
-        )
-        return c
-
-    lax.fori_loop(1, total, greet, 0)
-    masters[me, 0] = query_master[...].astype(jnp.bfloat16)
-    masters[me, 1] = out_master[...].astype(jnp.bfloat16)
-    pl.semaphore_wait(barrier, total - 1)
+            barrier, inc=1, device_id={"fs": f, "tp": tt}, device_id_type=MESH
+        )
+
+    def loop(low, high, act):
+        def go(i, c):
+            act(i)
+            return c
+        lax.fori_loop(low, high, go, 0)
+
+    shares = factors.shape[2]
+    if shares == tp // 2:
+        loop(1, nz, lambda i: greet(lax.rem(z + i, nz) * ny + y, t))
+        loop(1, ny, lambda i: greet(z * ny + lax.rem(y + i, ny), t))
+        loop(1, shares, lambda i: greet(me, lax.rem(t + 2 * i, tp)))
+        greet(me, other)
+        greeted = nz + ny + shares - 2
+    else:
+        loop(1, total, lambda i: greet(lax.rem(mine + i, total) // tp, lax.rem(mine + i, tp)))
+        greeted = total - 1
+    masters[0, me] = query_master[...].astype(jnp.bfloat16)
+    masters[1, me] = out_master[...].astype(jnp.bfloat16)
+    pl.semaphore_wait(barrier, greeted)
     own_factor(query_factor).wait()
 
     def remote(src, dst, send, recv, f, tt=None):
@@ -124,13 +145,7 @@
             piece(zz, src), piece(zz, src), sems[3].at[zz, dy], sems[4].at[zz, src], z * ny + src
         )
 
-    def loop(low, high, act):
-        def go(i, c):
-            act(i)
-            return c
-        lax.fori_loop(low, high, go, 0)
-
-    def hops(piece, low, high, sems, extra=None):
+    def hops(piece, low, high, sems):
         def pass_on(zz, come, up_too, down_too):
             @pl.when(come)
             def _():
@@ -147,8 +162,6 @@
                     down(piece, zz, sems).start()
 
                 loop(1, ny, lambda dy: along_y(piece, zz, dy, sems).start())
-                if extra is not None:
-                    extra(zz, y)
 
         def step(k):
             pass_on(z - k, z >= k, z < nz - 1, (k == 0) & (z > 0))
@@ -170,14 +183,16 @@
 
         all_y(lambda zz, dy: along_y(piece, zz, dy, sems).wait_send())
 
-    shares = factors.shape[2]
     part = lax.rem(t // 2, shares)
 
     def f_piece(zz, yy):
         return factors.at[core, zz * ny + yy, part]
 
-    def m_piece(zz, yy):
-        return masters.at[zz * ny + yy]
+    def q_piece(zz, yy):
+        return masters.at[0, zz * ny + yy]
+
+    def o_piece(zz, yy):
+        return masters.at[1, zz * ny + yy]
 
     def over_x(zz, yy, dx):
         block = zz * ny + yy
@@ -201,10 +216,50 @@
             for dx in range(1, shares):
                 over_x(zz, yy, dx).start()
 
-    f_sems = (fu_send, fd_send, fz_recv, fy_send, fy_recv)
-    m_sems = (mu_send, md_send, mz_recv, my_send, my_recv)
-    hops(f_piece, 0, nz, f_sems, send_x)
-    hops(m_piece, 0, 1, m_sems)
+    f_sems = (None, None, fz_recv, fy_send, fy_recv)
+    q_sems = (mu_send.at[0], md_send.at[0], mz_recv.at[0], my_send.at[0], my_recv.at[0])
+    o_sems = (mu_send.at[1], md_send.at[1], mz_recv.at[1], my_send.at[1], my_recv.at[1])
+
+    def m_hops(low, high):
+        def both(k):
+            hops(q_piece, k, k + 1, q_sems)
+            hops(o_piece, k, k + 1, o_sems)
+
+        loop(low, high, both)
+
+
+    def to_z(zz):
+        own_piece = f_piece(z, y)
+        return remote(own_piece, own_piece, fz_send.at[zz], fz_recv.at[z], zz * ny + y)
+
+    def of_z(zz):
+        piece = f_piece(zz, y)
+        return remote(piece, piece, fz_send.at[zz], fz_recv.at[zz], zz * ny + y)
+
+    def nearest(act):
+        def step(k):
+            @pl.when(z >= k)
+            def _():
+                act(z - k)
+
+            @pl.when(z + k < nz)
+            def _():
+                act(z + k)
+
+        loop(1, nz, step)
+
+    def pass_f(zz):
+        of_z(zz).wait_recv()
+        f_onward(zz)
+
+    def f_onward(zz):
+        loop(1, ny, lambda dy: along_y(f_piece, zz, dy, f_sems).start())
+        send_x(zz, y)
+
+    nearest(lambda zz: to_z(zz).start())
+    f_onward(z)
+    nearest(pass_f)
+    m_hops(0, 1)
     pltpu.make_async_copy(inputs, xbuf, local_sem.at[1]).wait()
 
     def take_y(zz, dy):
@@ -264,8 +319,10 @@
         lax.fori_loop(1, n, go, 0)
 
     each(scatter, lambda d: d.start())
-    hops(m_piece, 1, 2, m_sems)
+    m_hops(1, 3)
     each(scattered, lambda d: d.wait_recv())
+    back = factors.at[1 - core]
+    remote(back, back, fc_sem.at[0], fc_sem.at[1], me, other).wait_recv()
 
     got[me] = parts[me]
 
@@ -306,20 +363,21 @@
         return remote(dirs.at[f], dirs.at[f], ag_send.at[f], ag_recv.at[f], f)
 
     each(spread, lambda d: d.start())
-    hops(m_piece, 2, nz, m_sems)
+    m_hops(3, nz)
     each(arrived, lambda d: d.wait_recv())
     for w in range(2):
         for j in range(n):
             whole[j * own:(j + 1) * own, :] = dirs[j, w].astype(jnp.float32)
         direction[w] = whole[...].astype(jnp.bfloat16)
 
-    all_y(lambda zz, dy: from_y(m_piece, zz, dy, m_sems).wait_recv())
-    back = factors.at[1 - core]
-    remote(back, back, fc_sem.at[0], fc_sem.at[1], me, other).wait_recv()
+    all_y(lambda zz, dy: from_y(q_piece, zz, dy, q_sems).wait_recv())
+    all_y(lambda zz, dy: from_y(o_piece, zz, dy, o_sems).wait_recv())
     share.wait_send()
     swap.wait_send()
-    sent(f_piece, f_sems)
-    sent(m_piece, m_sems)
+    nearest(lambda zz: to_z(zz).wait_send())
+    all_y(lambda zz, dy: along_y(f_piece, zz, dy, f_sems).wait_send())
+    sent(q_piece, q_sems)
+    sent(o_piece, o_sems)
     others(lambda zz, yy, dx: over_x(zz, yy, dx).wait_send())
     each(scatter, lambda d: d.wait_send())
     each(spread, lambda d: d.wait_send())
@@ -339,13 +397,14 @@
     dma = pltpu.SemaphoreType.DMA
     bf, f32 = jnp.bfloat16, jnp.float32
     shares = shares_of(tp, rows)
-    gather = (dma((nz,)), dma((nz,)), dma((nz,)), dma((nz, ny)), dma((nz, ny)))
+    gather = (dma((nz,)), dma((nz,)), dma((nz, ny)), dma((nz, ny)))
+    chunks = (dma((2, nz)), dma((2, nz)), dma((2, nz)), dma((2, nz, ny)), dma((2, nz, ny)))
     shape = jax.ShapeDtypeStruct
     return pl.pallas_call(
         functools.partial(kernel, n, tp, 2.0 * rank * cols * tp),
         out_shape=(
             shape((2, n, shares, rows // shares, rank), bf),
-            shape((n, 2, rows, cols), bf),
+            shape((2, n, rows, cols), bf),
             shape((2, rank, cols), bf),
             shape((2, own, cols), f32),
         ),
@@ -362,7 +421,7 @@
             pltpu.VMEM((rank, cols), f32),
             dma((2,)), dma((2,)),
             *gather, dma((n, shares)), dma((n, shares)), dma((2,)),
-            *gather,
+            *chunks,
             dma((n,)), dma((n,)), dma((2,)), dma((n,)), dma((n,)),
         ],
         compiler_params=pltpu.CompilerParams(
@@ -395,13 +454,14 @@
     def fixed(*dims):
         return pl.BlockSpec(dims, lambda j: (0,) * len(dims))
 
-    block = pl.BlockSpec((rows, cols), lambda j: (j, 0))
+    blocks = n // math.gcd(n, 4)
+    block = pl.BlockSpec((blocks * rows, cols), lambda j: (j, 0))
     return pl.pallas_call(
         finish,
-        grid=(n,),
+        grid=(n // blocks,),
         in_specs=[
-            pl.BlockSpec((2, 1, rows, rank), lambda j: (0, j, 0, 0)),
-            pl.BlockSpec((1, 2, rows, cols), lambda j: (j, 0, 0, 0)),
+            pl.BlockSpec((2, blocks, rows, rank), lambda j: (0, j, 0, 0)),
+            pl.BlockSpec((2, blocks, rows, cols), lambda j: (0, j, 0, 0)),
             fixed(2, rank, cols),
             fixed(2, own, cols),
         ] + [fixed(own, cols)] * 4,

time: 75.7 us -> 67.9 us (0.90)
  Pallas kernels: 74.7 us -> 67.1 us
    pallas_call x1, Pallas kernels: 66.6 us -> 60.4 us  [exchange(): pl.pallas_call(functools.partial(kernel, n, tp, 2.0 * rank * cols * tp),...]
    pallas_call x1, Pallas kernels: 8.11 us -> 6.67 us  [body(): pl.pallas_call(finish, grid=(n // blocks,), in_specs=[pl.BlockSpec((2, bl...]
where the time goes in v3:
time: 67.9 us; the launch traced here: 67.7 us
  Pallas kernels  67.1 us (99%)
    pallas_call x1, Pallas kernels, exchange(): pl.pallas_call(functools.partial(kernel, n, tp, 2.0 * rank * cols * tp),...  60.4 us
    pallas_call x1, Pallas kernels, body(): pl.pallas_call(finish, grid=(n // blocks,), in_specs=[pl.BlockSpec((2, bl...  6.67 us

profile of v3, /device:TPU:0, one launch (start us, length us, event | category | flops | bytes accessed | tf_op | source)
XLA Modules:
  0.0 67.7 jit_solution(8704580880095367824)
XLA Ops:
  0.6 60.4 %shard_map.179 = (bf16[2,8,2,144,192]{4,3,2,1,0:T(8,128)(2,1)}, bf16[2,8,288,256]{3,2,1,0:T(8,128)(2,1)}, bf16[2,192,256]{2,1,0:T(8,128)(2,1)}, f32[2,24,256]{2,1,0:T(8,128)}) custom-call(bf16[1024,2304]{1,0:T(8,128)(2,1)} %inputs.1, bf16[1024,2304]{1,0:T(8,128)(2,1)} %out_cot.1, bf16[2,144,192]{2,1,0:T(8,128)(2,1)} %bitcast.4, ...), custom_call_target="tpu_custom_call" | custom-call | tf_op jit(solution)/shard_map/pallas_call | solution.py:403
  61.0 6.7 %shard_map.180 = (f32[288,256]{1,0:T(8,128)}, f32[288,256]{1,0:T(8,128)}, bf16[2304,256]{1,0:T(8,128)(2,1)}, bf16[2304,256]{1,0:T(8,128)(2,1)}, f32[24,256]{1,0:...) custom-call(bf16[2,8,288,192]{3,2,1,0:T(8,128)(2,1)} %bitcast.3, ...), custom_call_target="tpu_custom_call" | custom-call | tf_op jit(solution)/shard_map/pallas_call | solution.py:459

commit v4 on v3

--- a/solution.py
+++ b/solution.py
@@ -57,7 +57,19 @@
                 step_out[...] = step
         return c
 
-    lax.fori_loop(0, blocks, one, 0)
+    if rows % 16 == 0:
+        for w, (step_out, copy) in enumerate(((query_step, query_copy), (out_step, out_copy))):
+            step = jnp.dot(
+                factors[w].reshape(blocks * rows, -1), direction[w], preferred_element_type=jnp.float32
+            )
+            master = masters[w].reshape(blocks * rows, -1).astype(jnp.float32)
+            copy[...] = (master - learn_rate * step).astype(copy.dtype)
+            for i in range(blocks):
+                @pl.when(j * blocks + i == me)
+                def _():
+                    step_out[...] = step[i * rows:(i + 1) * rows]
+    else:
+        lax.fori_loop(0, blocks, one, 0)
 
 
 def kernel(
@@ -272,6 +284,7 @@
         for dx in range(1, shares):
             loop(1, n, lambda i: act(lax.rem(me + i, n) // ny, lax.rem(me + i, ny), dx))
 
+    m_hops(1, 2)
     others(lambda zz, yy, dx: from_x(zz, yy, dx).wait_recv())
     fac = factors.at[core]
     share = remote(fac, fac, fc_sem.at[0], fc_sem.at[1], me, other)
@@ -319,7 +332,7 @@
         lax.fori_loop(1, n, go, 0)
 
     each(scatter, lambda d: d.start())
-    m_hops(1, 3)
+    m_hops(2, nz)
     each(scattered, lambda d: d.wait_recv())
     back = factors.at[1 - core]
     remote(back, back, fc_sem.at[0], fc_sem.at[1], me, other).wait_recv()
@@ -363,7 +376,6 @@
         return remote(dirs.at[f], dirs.at[f], ag_send.at[f], ag_recv.at[f], f)
 
     each(spread, lambda d: d.start())
-    m_hops(3, nz)
     each(arrived, lambda d: d.wait_recv())
     for w in range(2):
         for j in range(n):
@@ -454,7 +466,7 @@
     def fixed(*dims):
         return pl.BlockSpec(dims, lambda j: (0,) * len(dims))
 
-    blocks = n // math.gcd(n, 4)
+    blocks = n // 2
     block = pl.BlockSpec((blocks * rows, cols), lambda j: (j, 0))
     return pl.pallas_call(
         finish,

time: 67.9 us -> 60.9 us (0.90)
  Pallas kernels: 67.1 us -> 60.1 us
    pallas_call x1, Pallas kernels: 60.4 us -> 55.2 us  [exchange(): pl.pallas_call(functools.partial(kernel, n, tp, 2.0 * rank * cols * tp),...]
    pallas_call x1, Pallas kernels: 6.67 us -> 4.85 us  [body(): pl.pallas_call(finish, grid=(n // blocks,), in_specs=[pl.BlockSpec((2, bl...]
where the time goes in v4:
time: 60.9 us; the launch traced here: 60.7 us
  Pallas kernels  60.1 us (99%)
  between operations  0.64 us (1%)
    pallas_call x1, Pallas kernels, exchange(): pl.pallas_call(functools.partial(kernel, n, tp, 2.0 * rank * cols * tp),...  55.2 us
    pallas_call x1, Pallas kernels, body(): pl.pallas_call(finish, grid=(n // blocks,), in_specs=[pl.BlockSpec((2, bl...  4.85 us

profile of v4, /device:TPU:0, one launch (start us, length us, event | category | flops | bytes accessed | tf_op | source)
XLA Modules:
  0.0 60.7 jit_solution(3769881935624061796)
XLA Ops:
  0.6 55.2 %shard_map.179 = (bf16[2,8,2,144,192]{4,3,2,1,0:T(8,128)(2,1)}, bf16[2,8,288,256]{3,2,1,0:T(8,128)(2,1)}, bf16[2,192,256]{2,1,0:T(8,128)(2,1)}, f32[2,24,256]{2,1,0:T(8,128)}) custom-call(bf16[1024,2304]{1,0:T(8,128)(2,1)} %inputs.1, bf16[1024,2304]{1,0:T(8,128)(2,1)} %out_cot.1, bf16[2,144,192]{2,1,0:T(8,128)(2,1)} %bitcast.4, ...), custom_call_target="tpu_custom_call" | custom-call | tf_op jit(solution)/shard_map/pallas_call | solution.py:415
  55.9 4.9 %shard_map.180 = (f32[288,256]{1,0:T(8,128)}, f32[288,256]{1,0:T(8,128)}, bf16[2304,256]{1,0:T(8,128)(2,1)}, bf16[2304,256]{1,0:T(8,128)(2,1)}, f32[24,256]{1,0:...) custom-call(bf16[2,8,288,192]{3,2,1,0:T(8,128)(2,1)} %bitcast.3, ...), custom_call_target="tpu_custom_call" | custom-call | tf_op jit(solution)/shard_map/pallas_call | solution.py:471

commit v5 on v4

--- a/solution.py
+++ b/solution.py
@@ -77,9 +77,9 @@
     inputs, out_cot, query_factor, out_factor,
     query_cot, head_out, query_master, out_master,
     query_first, query_second, out_first, out_second,
-    factors, masters, direction, normed_out,
-    xbuf, lows, terms, parts, got, squares, dirs, whole,
-    local_sem, low_sem, fz_send, fz_recv, fy_send, fy_recv, fx_send, fx_recv, fc_sem,
+    factors_out, masters_out, direction, normed_out,
+    factors, masters, cots, fulls, olds, xbuf, lows, terms, parts, got, squares, dirs, whole,
+    local_sem, in_sem, out_sem, low_sem, fz_send, fz_recv, fy_send, fy_recv, fx_send, fx_recv, fc_sem,
     mu_send, md_send, mz_recv, my_send, my_recv, rs_send, rs_recv, ss_sem, ag_send, ag_recv,
 ):
     nz, ny = split_axis(n)
@@ -127,8 +127,20 @@
     else:
         loop(1, total, lambda i: greet(lax.rem(mine + i, total) // tp, lax.rem(mine + i, tp)))
         greeted = total - 1
-    masters[0, me] = query_master[...].astype(jnp.bfloat16)
-    masters[1, me] = out_master[...].astype(jnp.bfloat16)
+    loads = [
+        pltpu.make_async_copy(source, target, in_sem.at[k])
+        for k, (source, target) in enumerate((
+            (query_master, fulls.at[0]), (out_master, fulls.at[1]),
+            (query_cot, cots.at[0]), (head_out, cots.at[1]),
+            (query_first, olds.at[0]), (query_second, olds.at[1]),
+            (out_first, olds.at[2]), (out_second, olds.at[3]),
+        ))
+    ]
+    for load in loads:
+        load.start()
+    for w in range(2):
+        loads[w].wait()
+        masters[w, me] = fulls[w].astype(jnp.bfloat16)
     pl.semaphore_wait(barrier, greeted)
     own_factor(query_factor).wait()
 
@@ -297,7 +309,7 @@
     else:
         table = factors[core].astype(jnp.float32).reshape(width, rank).astype(jnp.bfloat16)
     tokens = xbuf.shape[0]
-    tile = math.gcd(tokens, 256)
+    tile = math.gcd(tokens, 512)
 
     def fold(i, c):
         at = pl.ds(pl.multiple_of(i * tile, tile), tile)
@@ -311,8 +323,10 @@
     swap.start()
     swap.wait_recv()
 
-    terms[0] = lax.dot_general(lows[0], query_cot[...], contract_rows, preferred_element_type=jnp.float32)
-    terms[1] = lax.dot_general(lows[1], head_out[...], contract_rows, preferred_element_type=jnp.float32)
+    for load in loads[2:]:
+        load.wait()
+    terms[0] = lax.dot_general(lows[0], cots[0], contract_rows, preferred_element_type=jnp.float32)
+    terms[1] = lax.dot_general(lows[1], cots[1], contract_rows, preferred_element_type=jnp.float32)
     for j in range(n):
         for w in range(2):
             parts[j, w] = terms[w, j * own:(j + 1) * own, :].astype(jnp.bfloat16)
@@ -332,10 +346,12 @@
         lax.fori_loop(1, n, go, 0)
 
     each(scatter, lambda d: d.start())
-    m_hops(2, nz)
+    m_hops(2, 3)
     each(scattered, lambda d: d.wait_recv())
     back = factors.at[1 - core]
     remote(back, back, fc_sem.at[0], fc_sem.at[1], me, other).wait_recv()
+    put_factors = pltpu.make_async_copy(factors, factors_out, out_sem.at[0])
+    put_factors.start()
 
     got[me] = parts[me]
 
@@ -356,15 +372,15 @@
         return c
 
     lax.fori_loop(1, total, tell, 0)
+    m_hops(3, nz)
     rest = squares.at[pl.ds(0, total - 1)]
     pltpu.make_async_copy(rest, rest, ss_sem.at[1]).wait()
     rms = jnp.sqrt(jnp.sum(squares[...]) / count + norm_eps)
 
-    olds = ((query_first, query_second), (out_first, out_second))
     for w in range(2):
         normed = proj[w] / rms
         normed_out[w] = normed
-        first, second = moments(normed, olds[w][0][...], olds[w][1][...])
+        first, second = moments(normed, olds[2 * w], olds[2 * w + 1])
         dirs[me, w] = (first / (jnp.sqrt(second) + adam_eps)).astype(jnp.bfloat16)
 
     def spread(i):
@@ -383,7 +399,11 @@
         direction[w] = whole[...].astype(jnp.bfloat16)
 
     all_y(lambda zz, dy: from_y(q_piece, zz, dy, q_sems).wait_recv())
+    put_q = pltpu.make_async_copy(masters.at[0], masters_out.at[0], out_sem.at[1])
+    put_q.start()
     all_y(lambda zz, dy: from_y(o_piece, zz, dy, o_sems).wait_recv())
+    put_o = pltpu.make_async_copy(masters.at[1], masters_out.at[1], out_sem.at[2])
+    put_o.start()
     share.wait_send()
     swap.wait_send()
     nearest(lambda zz: to_z(zz).wait_send())
@@ -394,6 +414,9 @@
     each(scatter, lambda d: d.wait_send())
     each(spread, lambda d: d.wait_send())
     pltpu.make_async_copy(rest, rest, ss_sem.at[0]).wait()
+    put_factors.wait()
+    put_q.wait()
+    put_o.wait()
 
 
 def exchange(n, tp, inputs, out_cot, query_factor, out_factor, query_cot, head_out,
@@ -420,9 +443,14 @@
             shape((2, rank, cols), bf),
             shape((2, own, cols), f32),
         ),
-        in_specs=[anyspace] * 4 + [vmem] * 8,
-        out_specs=(vmem,) * 4,
+        in_specs=[anyspace] * 12,
+        out_specs=(anyspace, anyspace, vmem, vmem),
         scratch_shapes=[
+            pltpu.VMEM((2, n, shares, rows // shares, rank), bf),
+            pltpu.VMEM((2, n, rows, cols), bf),
+            pltpu.VMEM((2, tokens, cols), bf),
+            pltpu.VMEM((2, rows, cols), f32),
+            pltpu.VMEM((4, own, cols), f32),
             pltpu.VMEM((tokens, width), bf),
             pltpu.VMEM((2, tokens, rank), bf),
             pltpu.VMEM((2, rank, cols), f32),
@@ -431,7 +459,7 @@
             pltpu.VMEM((n * tp, 1, 128), f32),
             pltpu.VMEM((n, 2, own, cols), bf),
             pltpu.VMEM((rank, cols), f32),
-            dma((2,)), dma((2,)),
+            dma((2,)), dma((8,)), dma((3,)), dma((2,)),
             *gather, dma((n, shares)), dma((n, shares)), dma((2,)),
             *chunks,
             dma((n,)), dma((n,)), dma((2,)), dma((n,)), dma((n,)),

time: 60.9 us -> 57.6 us (0.946)
  Pallas kernels: 60.1 us -> 56.8 us
    pallas_call x1, Pallas kernels: 55.2 us -> 52 us  [exchange(): pl.pallas_call(functools.partial(kernel, n, tp, 2.0 * rank * cols * tp),...]
where the time goes in v5:
time: 57.6 us; the launch traced here: 57.4 us
  Pallas kernels  56.8 us (99%)
  between operations  0.64 us (1%)
    pallas_call x1, Pallas kernels, exchange(): pl.pallas_call(functools.partial(kernel, n, tp, 2.0 * rank * cols * tp),...  52 us
    pallas_call x1, Pallas kernels, body(): pl.pallas_call(finish, grid=(n // blocks,), in_specs=[pl.BlockSpec((2, bl...  4.85 us

profile of v5, /device:TPU:0, one launch (start us, length us, event | category | flops | bytes accessed | tf_op | source)
XLA Modules:
  0.0 57.4 jit_solution(1975311507405925945)
XLA Ops:
  0.6 52.0 %shard_map.179 = (bf16[2,8,2,144,192]{4,3,2,1,0:T(8,128)(2,1)}, bf16[2,8,288,256]{3,2,1,0:T(8,128)(2,1)}, bf16[2,192,256]{2,1,0:T(8,128)(2,1)}, f32[2,24,256]{2,1,0:T(8,128)}) custom-call(bf16[1024,2304]{1,0:T(8,128)(2,1)} %inputs.1, bf16[1024,2304]{1,0:T(8,128)(2,1)} %out_cot.1, bf16[2,144,192]{2,1,0:T(8,128)(2,1)} %bitcast.4, ...), custom_call_target="tpu_custom_call" | custom-call | tf_op jit(solution)/shard_map/pallas_call | solution.py:438
  52.6 4.9 %shard_map.180 = (f32[288,256]{1,0:T(8,128)}, f32[288,256]{1,0:T(8,128)}, bf16[2304,256]{1,0:T(8,128)(2,1)}, bf16[2304,256]{1,0:T(8,128)(2,1)}, f32[24,256]{1,0:...) custom-call(bf16[2,8,288,192]{3,2,1,0:T(8,128)(2,1)} %bitcast.3, ...), custom_call_target="tpu_custom_call" | custom-call | tf_op jit(solution)/shard_map/pallas_call | solution.py:499
